TPU v7x, 32 devices: a whole 2x2x4 slice. The times are simulated.
32 devices in a mesh: grp: 2 (over x), tp: 4 (over y, core), dp: 4 (over z).
Axes of the slice: x: 2, y: 2, z: 4, core: 2. Of those that a mesh axis runs over, the one named last changes fastest.
Arguments:
- tokens: bfloat16 [512, 2048], P(('grp', 'tp'), 'dp'), parts along dimension 0, may hold values from -25 to 25
- state: float32 [2, 512, 16, 128, 128], P(None, ('grp', 'dp'), 'tp'), parts along dimension 1, may hold values from -1 to 1
- lengths: int32 [512], P(('grp', 'dp')), parts along dimension 0, may hold values from 1 to 4096, 131072 in all
- norm_gain: bfloat16 [2, 2048], P(None, 'dp'), may hold values from 0.099609375 to 1.8984375
- w_query: bfloat16 [2, 2048, 2048], P(None, 'dp', 'tp'), may hold values from -0.125 to 0.125
- w_forget: bfloat16 [2, 2048, 2048], P(None, 'dp', 'tp'), may hold values from -0.125 to 0.125
- w_input: bfloat16 [2, 2048, 2048], P(None, 'dp', 'tp'), may hold values from -0.125 to 0.125
- w_gate: bfloat16 [2, 2048, 2048], P(None, 'dp', 'tp'), may hold values from -0.125 to 0.125
- w_out: bfloat16 [2, 2048, 2048], P(None, 'tp', 'dp'), may hold values from -0.125 to 0.125
- bound_logit: float32 [2, 2048], P(None, 'tp'), may hold values from -3 to 5
- pace: float32 [2, 2048], P(None, 'tp'), may hold values from 0.6 to 2
- head_gain: float32 [2, 128], replicated, may hold values from 0.4 to 2.5
Outputs:
- mixed: float32 [512, 2048], P(('grp', 'tp'), 'dp'), parts along dimension 0
- new_state: float32 [2, 512, 16, 128, 128], P(None, ('grp', 'dp'), 'tp'), parts along dimension 1
There are 2 independent parts, one for each index of `grp`. A program takes and returns all parts, laid end to end along the dimension named above; an argument that names none is the same for every part. Nothing has to cross between parts.
All inputs are finite; a program needn't handle non-finite values. No bound on the sum of `lengths` on one device may be relied on, other than what follows from the above.
Results may differ from a plain program's by a relative error of at most 0.0083.
Values may be sent and summed in bfloat16 or wider, within the bound.
A program may use at most 192 MiB of HBM per device.

v0:
```python
import jax
import jax.numpy as jnp
from jax import lax
from jax.sharding import PartitionSpec as P

D = 2048
LENGTH_MEAN = 512
epsilon = 1e-06


def advance(prior, query, forget_in, value, gate, lower, pace_row, log_len, gain_row):
    count, width = query.shape
    size = prior.shape[-1]
    heads = width // size
    pre = forget_in - pace_row[None, :] * log_len[:, None]
    forget = lower[None, :] + (1.0 - lower[None, :]) * jax.nn.sigmoid(pre)
    key = (1.0 - lower[None, :]) * jax.nn.sigmoid(-pre)
    forget = forget.reshape(count, heads, size)
    key = key.reshape(count, heads, size)
    values = value.reshape(count, heads, size)
    updated = forget[..., None] * prior + key[..., None] * values[:, :, None, :]
    readout = jnp.einsum(
        "bhk,bhkv->bhv", query.reshape(count, heads, size), updated, precision=lax.Precision.HIGHEST
    )
    normed = readout * lax.rsqrt(jnp.mean(readout * readout, axis=-1, keepdims=True) + epsilon)
    gates = gate.reshape(count, heads, size)
    normed = normed * gain_row[None, None, :] * jax.nn.silu(gates)
    return (updated, normed.reshape(count, width).astype(jnp.bfloat16))


def shards(
    tokens,
    state,
    lengths,
    norm_gain,
    w_query,
    w_forget,
    w_input,
    w_gate,
    w_out,
    bound_logit,
    pace,
    head_gain,
):
    current = tokens
    log_len = jnp.log(lengths.astype(jnp.float32) / LENGTH_MEAN)
    own_count = state.shape[1]
    states = []
    result = None
    for block in range(2):
        whole = lax.all_gather(current, "tp", axis=0, tiled=True)
        whole_wide = whole.astype(jnp.float32)
        partial_sq = jnp.sum(whole_wide * whole_wide, axis=1)
        squares_all = lax.psum(partial_sq, "dp")
        squares = lax.dynamic_slice_in_dim(
            squares_all, lax.axis_index("dp") * own_count, own_count, 0
        )
        gained = (whole_wide * norm_gain[block].astype(jnp.float32)[None, :]).astype(jnp.bfloat16)
        terms = tuple(
            (
                jnp.dot(gained, weight[block], preferred_element_type=jnp.float32)
                for weight in (w_query, w_forget, w_input, w_gate)
            )
        )
        sums = lax.psum_scatter(terms, "dp", scatter_dimension=0, tiled=True)
        scale = lax.rsqrt(squares / D + epsilon)
        made = [scale[:, None] * total for total in sums]
        lower = jax.nn.sigmoid(bound_logit[block])
        updated, normed = advance(
            state[block],
            made[0],
            made[1],
            made[2],
            made[3],
            lower,
            pace[block],
            log_len,
            head_gain[block],
        )
        states.append(updated)
        gathered = lax.all_gather(normed, "dp", axis=0, tiled=True)
        out_weight = w_out[block]
        branch = lax.psum_scatter(
            jnp.dot(gathered, out_weight, preferred_element_type=jnp.float32),
            "tp",
            scatter_dimension=0,
            tiled=True,
        )
        if block == 0:
            current = (current.astype(jnp.float32) + branch).astype(jnp.bfloat16)
        else:
            result = current.astype(jnp.float32) + branch
    return (result, jnp.stack(states))


def solution(mesh):
    in_specs = (
        P(("grp", "tp"), "dp"),
        P(None, ("grp", "dp"), "tp", None, None),
        P(("grp", "dp")),
        P(None, "dp"),
        P(None, "dp", "tp"),
        P(None, "dp", "tp"),
        P(None, "dp", "tp"),
        P(None, "dp", "tp"),
        P(None, "tp", "dp"),
        P(None, "tp"),
        P(None, "tp"),
        P(),
    )
    out_specs = (P(("grp", "tp"), "dp"), P(None, ("grp", "dp"), "tp", None, None))
    return jax.shard_map(shards, mesh=mesh, in_specs=in_specs, out_specs=out_specs, check_vma=False)
```

profile of v0, /device:TPU:0, one launch (start us, length us, event | category | flops | bytes accessed | tf_op | source)
XLA Modules:
  0.0 361.6 jit_solution(16375477499638168452)
XLA Ops:
  8.0 7.4 %all_gather.12 = bf16[256,512]{1,0:T(8,128)(2,1)S(1)} all-gather(bf16[64,512]{1,0:T(8,128)(2,1)} %param.12), channel_id=1, replica_groups=mesh['grp'=2,'tp'=4,'dp'=4] {'tp'}, dimensions={0}, use_global_device_ids=true | all-gather | bytes 327680 | tf_op jit(solution)/shard_map/all_gather | solution.py:51
  15.4 2.1 fusion.36
  17.6 2.1 fusion.34
  19.8 2.2 fusion.32
  22.1 2.2 fusion.38
  24.5 12.0 %psum.14 = f32[256]{0:T(256)S(1)} all-reduce(f32[256]{0:T(256)S(1)} %fusion.16), channel_id=1, replica_groups=mesh['grp'=2,'tp'=4,'dp'=4] {'dp'}, use_global_device_ids=true, to_apply=%region_1.0 | all-reduce | flops 256 | bytes 2048 | tf_op jit(solution)/shard_map/psum | solution.py:54
  40.9 22.4 %reduce-scatter.15.cloned.1.call-done = f32[64,512]{1,0:T(8,128)} async-done(((f32[256,512]{1,0:T(8,128)}), f32[64,512]{1,0:T(8,128)}) %reduce-scatter.15.cloned.1.call-update) | async-done | bytes 131088 | tf_op jit(solution)/shard_map/reduce_scatter | solution.py:65
  63.4 22.4 %reduce-scatter.17.cloned.1.call-done = f32[64,512]{1,0:T(8,128)} async-done(((f32[256,512]{1,0:T(8,128)}), f32[64,512]{1,0:T(8,128)}) %reduce-scatter.17.cloned.1.call-update) | async-done | bytes 131088 | tf_op jit(solution)/shard_map/reduce_scatter | solution.py:65
  85.8 22.2 %reduce-scatter.11.cloned.1.call-done = f32[64,512]{1,0:T(8,128)} async-done(((f32[256,512]{1,0:T(8,128)}), f32[64,512]{1,0:T(8,128)}) %reduce-scatter.11.cloned.1.call-update) | async-done | bytes 131088 | tf_op jit(solution)/shard_map/reduce_scatter | solution.py:65
  110.9 22.7 %fusion.4 = f32[64,4,1,128]{3,2,1,0:T(1,128)S(1)} fusion(f32[64,4,128,1]{2,3,1,0:T(1,128)} %bitcast.79, f32[2,64,4,128,128]{4,3,2,1,0:T(8,128)} %param.13, f32[64,4,128]{2,1,0:T(4,128)S(1)} %mul.316, f32[64,4,128]{2,1,0:T(4,128)S(1)} %mul.313, f32[64,4,128]{2,1,0:T(4,128)S(1)} %mul.309), kind=kOutput, calls=%fused_computation.6 | convolution fusion | flops 62914560 | bytes 17432576 | tf_op jit(solution)/shard_map/bhk,bhkv->bhv/dot_general | solution.py:22
  134.0 13.8 %all_gather.13 = bf16[256,512]{1,0:T(8,128)(2,1)S(1)} all-gather(bf16[64,512]{1,0:T(8,128)(2,1)S(1)} %bitcast.74), channel_id=1, replica_groups=mesh['grp'=2,'tp'=4,'dp'=4] {'dp'}, dimensions={0}, use_global_device_ids=true | all-gather | bytes 327680 | tf_op jit(solution)/shard_map/all_gather | solution.py:81
  147.8 2.1 fusion.30
  150.0 19.9 %reduce-scatter.19.cloned.1.call-done = f32[64,512]{1,0:T(8,128)} async-done(((f32[256,512]{1,0:T(8,128)}), f32[64,512]{1,0:T(8,128)}) %reduce-scatter.19.cloned.1.call-update) | async-done | bytes 131088 | tf_op jit(solution)/shard_map/reduce_scatter | solution.py:83
  170.9 5.8 %all_gather.14 = bf16[256,512]{1,0:T(8,128)(2,1)S(1)} all-gather(bf16[64,512]{1,0:T(8,128)(2,1)S(1)} %add_convert_fusion), channel_id=1, replica_groups=mesh['grp'=2,'tp'=4,'dp'=4] {'tp'}, dimensions={0}, use_global_device_ids=true | all-gather | bytes 327680 | tf_op jit(solution)/shard_map/all_gather | solution.py:51
  180.2 2.2 fusion.28
  182.6 11.7 %psum.15 = f32[256]{0:T(256)S(1)} all-reduce(f32[256]{0:T(256)S(1)} %fusion.18), channel_id=1, replica_groups=mesh['grp'=2,'tp'=4,'dp'=4] {'dp'}, use_global_device_ids=true, to_apply=%region_9.10 | all-reduce | flops 256 | bytes 2048 | tf_op jit(solution)/shard_map/psum | solution.py:54
  194.4 5.5 %reduce-scatter.23.cloned.1.call-done = f32[64,512]{1,0:T(8,128)} async-done(((f32[256,512]{1,0:T(8,128)}), f32[64,512]{1,0:T(8,128)}) %reduce-scatter.23.cloned.1.call-update) | async-done | bytes 131088 | tf_op jit(solution)/shard_map/reduce_scatter | solution.py:65
  199.9 22.4 %reduce-scatter.25.cloned.1.call-done = f32[64,512]{1,0:T(8,128)} async-done(((f32[256,512]{1,0:T(8,128)}), f32[64,512]{1,0:T(8,128)}) %reduce-scatter.25.cloned.1.call-update) | async-done | bytes 131088 | tf_op jit(solution)/shard_map/reduce_scatter | solution.py:65
  222.3 22.4 %reduce-scatter.27.cloned.1.call-done = f32[64,512]{1,0:T(8,128)} async-done(((f32[256,512]{1,0:T(8,128)}), f32[64,512]{1,0:T(8,128)}) %reduce-scatter.27.cloned.1.call-update) | async-done | bytes 131088 | tf_op jit(solution)/shard_map/reduce_scatter | solution.py:65
  244.7 22.4 %reduce-scatter.21.cloned.1.call-done = f32[64,512]{1,0:T(8,128)} async-done(((f32[256,512]{1,0:T(8,128)}), f32[64,512]{1,0:T(8,128)}) %reduce-scatter.21.cloned.1.call-update) | async-done | bytes 131088 | tf_op jit(solution)/shard_map/reduce_scatter | solution.py:65
  268.6 23.2 %multiply_add_fusion.1 = (f32[1,64,4,128,128]{4,3,2,1,0:T(8,128)}, f32[1,64,4,128,128]{4,3,2,1,0:T(8,128)}) fusion(f32[2,64,4,128,128]{4,3,2,1,0:T(8,128)} %param.13, f32[64,4,128]{2,1,0:T(4,128)} %copy-done.6, f32[64,4,128]{2,1,0:T(4,128)} %copy-done.5, f32[64,4,128]{2,1,0:T(4,128)} %copy-done.4, f32[64,4,128]{2,1,0:T(4,128)S(1)} %mul.349, ...), kind=kLoop, calls=%fused_computation.8 | loop fusion | flops 25165824 | bytes 67895296 | tf_op jit(solution)/shard_map/add | solution.py:21
  291.8 22.6 %fusion.1 = f32[64,4,1,128]{3,2,1,0:T(1,128)S(1)} fusion(f32[64,4,128,1]{2,3,1,0:T(1,128)S(1)} %bitcast.78, f32[2,64,4,128,128]{4,3,2,1,0:T(8,128)} %param.13, f32[64,4,128]{2,1,0:T(4,128)S(1)} %mul.349, f32[64,4,128]{2,1,0:T(4,128)S(1)} %mul.346, f32[64,4,128]{2,1,0:T(4,128)S(1)} %mul.342), kind=kOutput, calls=%fused_computation.3 | convolution fusion | flops 62914560 | bytes 17432576 | tf_op jit(solution)/shard_map/bhk,bhkv->bhv/dot_general | solution.py:22
  314.8 13.8 %all_gather.15 = bf16[256,512]{1,0:T(8,128)(2,1)S(1)} all-gather(bf16[64,512]{1,0:T(8,128)(2,1)S(1)} %bitcast.75), channel_id=1, replica_groups=mesh['grp'=2,'tp'=4,'dp'=4] {'dp'}, dimensions={0}, use_global_device_ids=true | all-gather | bytes 327680 | tf_op jit(solution)/shard_map/all_gather | solution.py:81
  329.7 23.4 %pad_maximum_fusion = f32[2,64,4,128,128]{4,3,2,1,0:T(8,128)} fusion(f32[1,64,4,128,128]{4,3,2,1,0:T(8,128)} %get-tuple-element.7, f32[1,64,4,128,128]{4,3,2,1,0:T(8,128)} %get-tuple-element.6), kind=kLoop, calls=%fused_computation | loop fusion | flops 8388608 | bytes 67108864 | tf_op jit(solution)/shard_map/stack | solution.py:93
  (79 shorter events, 18.0 us)
Async XLA Ops:
  7.2 33.7 %reduce-scatter.13.cloned.1.call-start = ((), (), s32[]{:S(2)}) async-start(), calls=%async_computation.11 | async-start | bytes 655360 | tf_op jit(solution)/shard_map/reduce_scatter | solution.py:65
  17.6 45.8 %reduce-scatter.15.cloned.1.call-start = ((), (), s32[]{:S(2)}) async-start(), calls=%async_computation.12 | async-start | bytes 655360 | tf_op jit(solution)/shard_map/reduce_scatter | solution.py:65
  19.8 66.0 %reduce-scatter.17.cloned.1.call-start = ((), (), s32[]{:S(2)}) async-start(), calls=%async_computation.13 | async-start | bytes 655360 | tf_op jit(solution)/shard_map/reduce_scatter | solution.py:65
  22.0 86.0 %reduce-scatter.11.cloned.1.call-start = ((), (), s32[]{:S(2)}) async-start(), calls=%async_computation.10 | async-start | bytes 655360 | tf_op jit(solution)/shard_map/reduce_scatter | solution.py:65
  24.3 145.7 %reduce-scatter.19.cloned.1.call-start = ((), (), s32[]{:S(2)}) async-start(), calls=%async_computation.14 | async-start | bytes 655360 | tf_op jit(solution)/shard_map/reduce_scatter | solution.py:83
  37.2 73.7 %copy-start.8 = (f32[64]{0:T(128)}, f32[64]{0:T(128)S(1)}, u32[]{:S(2)}) copy-start(f32[64]{0:T(128)S(1)} %multiply_log_fusion) | copy-start | bytes 772
  109.3 24.6 %copy-start.4 = (f32[64,4,128]{2,1,0:T(4,128)}, f32[64,4,128]{2,1,0:T(4,128)S(1)}, u32[]{:S(2)}) copy-start(f32[64,4,128]{2,1,0:T(4,128)S(1)} %mul.309) | copy-start | bytes 393220
  109.4 24.6 %copy-start.5 = (f32[64,4,128]{2,1,0:T(4,128)}, f32[64,4,128]{2,1,0:T(4,128)S(1)}, u32[]{:S(2)}) copy-start(f32[64,4,128]{2,1,0:T(4,128)S(1)} %mul.313) | copy-start | bytes 393220
  109.5 40.5 %copy-start.6 = (f32[64,4,128]{2,1,0:T(4,128)}, f32[64,4,128]{2,1,0:T(4,128)S(1)}, u32[]{:S(2)}) copy-start(f32[64,4,128]{2,1,0:T(4,128)S(1)} %mul.316) | copy-start | bytes 393220
  110.9 22.9 %copy-start.7 = (f32[64,4,128]{2,1,0:T(4,128)S(1)}, f32[64,4,128]{2,1,0:T(4,128)}, u32[]{:S(2)}) copy-start(f32[64,4,128]{2,1,0:T(4,128)} %reshape.56) | copy-start | bytes 393220
  110.9 22.9 %copy-start.10 = (f32[128]{0:T(128)S(1)}, f32[128]{0:T(128)}, u32[]{:S(2)}) copy-start(f32[128]{0:T(128)} %get-tuple-element.19) | copy-start | bytes 1540
  110.9 65.8 %copy-start = (bf16[2,512,512]{2,1,0:T(8,128)(2,1)S(1)}, bf16[2,512,512]{2,1,0:T(8,128)(2,1)}, u32[]{:S(2)}) copy-start(bf16[2,512,512]{2,1,0:T(8,128)(2,1)} %param.17) | copy-start | bytes 3145732
  110.9 66.9 %copy-start.1 = (bf16[2,512,512]{2,1,0:T(8,128)(2,1)S(1)}, bf16[2,512,512]{2,1,0:T(8,128)(2,1)}, u32[]{:S(2)}) copy-start(bf16[2,512,512]{2,1,0:T(8,128)(2,1)} %param.18) | copy-start | bytes 3145732
  110.9 68.1 %copy-start.2 = (bf16[2,512,512]{2,1,0:T(8,128)(2,1)S(1)}, bf16[2,512,512]{2,1,0:T(8,128)(2,1)}, u32[]{:S(2)}) copy-start(bf16[2,512,512]{2,1,0:T(8,128)(2,1)} %param.19) | copy-start | bytes 3145732
  150.0 49.9 %reduce-scatter.23.cloned.1.call-start = ((), (), s32[]{:S(2)}) async-start(), calls=%async_computation.16 | async-start | bytes 655360 | tf_op jit(solution)/shard_map/reduce_scatter | solution.py:65
  177.8 44.5 %reduce-scatter.25.cloned.1.call-start = ((), (), s32[]{:S(2)}) async-start(), calls=%async_computation.17 | async-start | bytes 655360 | tf_op jit(solution)/shard_map/reduce_scatter | solution.py:65
  178.9 65.7 %reduce-scatter.27.cloned.1.call-start = ((), (), s32[]{:S(2)}) async-start(), calls=%async_computation.18 | async-start | bytes 655360 | tf_op jit(solution)/shard_map/reduce_scatter | solution.py:65
  180.1 86.9 %reduce-scatter.21.cloned.1.call-start = ((), (), s32[]{:S(2)}) async-start(), calls=%async_computation.15 | async-start | bytes 655360 | tf_op jit(solution)/shard_map/reduce_scatter | solution.py:65
  182.4 170.8 %reduce-scatter.29.cloned.1.call-start = ((), (), s32[]{:S(2)}) async-start(), calls=%async_computation.19 | async-start | bytes 655360 | tf_op jit(solution)/shard_map/reduce_scatter | solution.py:83
  291.8 22.8 %copy-start.9 = (f32[128]{0:T(128)S(1)}, f32[128]{0:T(128)}, u32[]{:S(2)}) copy-start(f32[128]{0:T(128)} %get-tuple-element.18) | copy-start | bytes 1540
  291.8 36.8 %copy-start.3 = (bf16[2,512,512]{2,1,0:T(8,128)(2,1)S(1)}, bf16[2,512,512]{2,1,0:T(8,128)(2,1)}, u32[]{:S(2)}) copy-start(bf16[2,512,512]{2,1,0:T(8,128)(2,1)} %param.20) | copy-start | bytes 3145732
Sparse Core Ops, SparseCore 0:
  17.7 23.1 reduce-scatter.12
  43.2 20.1 reduce-scatter.14
  65.6 20.1 reduce-scatter.16
  87.9 20.0 reduce-scatter.10
  150.1 19.8 reduce-scatter.18
  177.9 21.9 reduce-scatter.22
  202.2 20.0 reduce-scatter.24
  224.6 20.0 reduce-scatter.26
  247.0 20.0 reduce-scatter.20
  329.8 19.8 reduce-scatter.28
where the time goes:
time: 362 us
  waiting for transfers between devices  161 us (44%)
  blocking collectives  64.5 us (18%)
  matrix products  62.6 us (17%)
  other arithmetic  54.8 us (15%)
  between operations  14.5 us (4%)
  local copies, waits for them, and re-layouts  3.97 us (1%)
    reduce_scatter x8, waiting for transfers between devices, shards(): sums = lax.psum_scatter(terms, 'dp', scatter_dimension=0, tiled=True)  141 us
    dot_general x2, matrix products, advance(): jnp.einsum('bhk,bhkv->bhv', query.reshape(count, heads, size), updated, p...  45.3 us
    all_gather x2, blocking collectives, shards(): gathered = lax.all_gather(normed, 'dp', axis=0, tiled=True)  27.6 us
    psum x2, blocking collectives, shards(): squares_all = lax.psum(partial_sq, 'dp')  23.7 us
    another operation x1, other arithmetic, shards(): return (result, jnp.stack(states))  23.4 us
    add x1, other arithmetic, advance(): updated = forget[..., None] * prior + key[..., None] * values[:, :, None, :]  23.2 us
    reduce_scatter x2, waiting for transfers between devices, shards(): lax.psum_scatter(jnp.dot(gathered, out_weight, preferred_element_type=jnp...  19.9 us
    dot_general x8, matrix products, shards(): jnp.dot(gained, weight[block], preferred_element_type=jnp.float32)  14.1 us
  transfers between devices with their start and end apart: 10, of which 9 were waited for; matrix products, arithmetic and copies ran while one was open for 11% of the time, Pallas kernels for 0%

commit v1 on v0

--- a/solution.py
+++ b/solution.py
@@ -78,7 +78,9 @@
             head_gain[block],
         )
         states.append(updated)
-        gathered = lax.all_gather(normed, "dp", axis=0, tiled=True)
+        gathered = jnp.concatenate(
+            lax.all_to_all(jnp.stack([normed] * lax.axis_size("dp")), "dp", 0, 0), axis=0
+        )
         out_weight = w_out[block]
         branch = lax.psum_scatter(
             jnp.dot(gathered, out_weight, preferred_element_type=jnp.float32),

time: 362 us -> 349 us (0.964)
  blocking collectives: 64.5 us -> 47.1 us
    all_gather x2 -> x0, blocking collectives: 27.6 us -> none  [shards(): gathered = lax.all_gather(normed, 'dp', axis=0, tiled=True)]
    all_to_all x0 -> x1, blocking collectives: none -> 10.1 us  [shards(): lax.all_to_all(jnp.stack([normed] * lax.axis_size('dp')), 'dp', 0, 0)]
  transfers between devices with their start and end apart: 10 -> 11, of which waited for: 9 -> 9; matrix products, arithmetic and copies ran while one was open for 11% -> 18% of each run, Pallas kernels for 0% -> 0%
where the time goes in v1:
time: 349 us
  waiting for transfers between devices  162 us (46%)
  matrix products  62.5 us (18%)
  other arithmetic  54.6 us (16%)
  blocking collectives  47.1 us (13%)
  between operations  14.5 us (4%)
  local copies, waits for them, and re-layouts  4.64 us (1%)
  starting transfers between devices  3.82 us (1%)
    reduce_scatter x8, waiting for transfers between devices, shards(): sums = lax.psum_scatter(terms, 'dp', scatter_dimension=0, tiled=True)  141 us
    dot_general x2, matrix products, advance(): jnp.einsum('bhk,bhkv->bhv', query.reshape(count, heads, size), updated, p...  45.2 us
    psum x2, blocking collectives, shards(): squares_all = lax.psum(partial_sq, 'dp')  23.7 us
    another operation x1, other arithmetic, shards(): return (result, jnp.stack(states))  23.4 us
    add x1, other arithmetic, advance(): updated = forget[..., None] * prior + key[..., None] * values[:, :, None, :]  23 us
    reduce_scatter x2, waiting for transfers between devices, shards(): lax.psum_scatter(jnp.dot(gathered, out_weight, preferred_element_type=jnp...  20.6 us
    dot_general x8, matrix products, shards(): jnp.dot(gained, weight[block], preferred_element_type=jnp.float32)  14 us
    all_gather x2, blocking collectives, shards(): whole = lax.all_gather(current, 'tp', axis=0, tiled=True)  13.2 us
  transfers between devices with their start and end apart: 11, of which 9 were waited for; matrix products, arithmetic and copies ran while one was open for 18% of the time, Pallas kernels for 0%

profile of v1, /device:TPU:0, one launch (start us, length us, event | category | flops | bytes accessed | tf_op | source)
XLA Modules:
  0.0 348.6 jit_solution(3910906539653043264)
XLA Ops:
  8.0 7.4 %all_gather.6 = bf16[256,512]{1,0:T(8,128)(2,1)S(1)} all-gather(bf16[64,512]{1,0:T(8,128)(2,1)} %param.12), channel_id=1, replica_groups=mesh['grp'=2,'tp'=4,'dp'=4] {'tp'}, dimensions={0}, use_global_device_ids=true | all-gather | bytes 327680 | tf_op jit(solution)/shard_map/all_gather | solution.py:51
  15.4 2.1 fusion.36
  17.6 2.1 fusion.34
  19.8 2.1 fusion.32
  22.1 2.2 fusion.38
  24.4 12.0 %psum.14 = f32[256]{0:T(256)S(1)} all-reduce(f32[256]{0:T(256)S(1)} %fusion.16), channel_id=1, replica_groups=mesh['grp'=2,'tp'=4,'dp'=4] {'dp'}, use_global_device_ids=true, to_apply=%region_1.0 | all-reduce | flops 256 | bytes 2048 | tf_op jit(solution)/shard_map/psum | solution.py:54
  40.9 22.4 %reduce-scatter.15.cloned.1.call-done = f32[64,512]{1,0:T(8,128)} async-done(((f32[256,512]{1,0:T(8,128)}), f32[64,512]{1,0:T(8,128)}) %reduce-scatter.15.cloned.1.call-update) | async-done | bytes 131088 | tf_op jit(solution)/shard_map/reduce_scatter | solution.py:65
  63.4 22.4 %reduce-scatter.17.cloned.1.call-done = f32[64,512]{1,0:T(8,128)} async-done(((f32[256,512]{1,0:T(8,128)}), f32[64,512]{1,0:T(8,128)}) %reduce-scatter.17.cloned.1.call-update) | async-done | bytes 131088 | tf_op jit(solution)/shard_map/reduce_scatter | solution.py:65
  85.8 22.2 %reduce-scatter.11.cloned.1.call-done = f32[64,512]{1,0:T(8,128)} async-done(((f32[256,512]{1,0:T(8,128)}), f32[64,512]{1,0:T(8,128)}) %reduce-scatter.11.cloned.1.call-update) | async-done | bytes 131088 | tf_op jit(solution)/shard_map/reduce_scatter | solution.py:65
  110.9 22.7 %fusion.4 = f32[64,4,1,128]{3,2,1,0:T(1,128)S(1)} fusion(f32[64,4,128,1]{2,3,1,0:T(1,128)} %bitcast.82, f32[2,64,4,128,128]{4,3,2,1,0:T(8,128)} %param.13, f32[64,4,128]{2,1,0:T(4,128)S(1)} %mul.316, f32[64,4,128]{2,1,0:T(4,128)S(1)} %mul.313, f32[64,4,128]{2,1,0:T(4,128)S(1)} %mul.309), kind=kOutput, calls=%fused_computation.6 | convolution fusion | flops 62914560 | bytes 17432576 | tf_op jit(solution)/shard_map/bhk,bhkv->bhv/dot_general | solution.py:22
  134.0 10.1 %all_to_all.10 = bf16[4,64,512]{2,1,0:T(8,128)(2,1)S(1)} all-to-all(bf16[4,64,512]{2,1,0:T(8,128)(2,1)S(1)} %stack.6), channel_id=1, replica_groups=mesh['grp'=2,'tp'=4,'dp'=4] {'dp'}, dimensions={0} | all-to-all | bytes 524288 | tf_op jit(solution)/shard_map/all_to_all | solution.py:82
  144.1 2.1 fusion.30
  146.4 20.6 %reduce-scatter.19.cloned.1.call-done = f32[64,512]{1,0:T(8,128)} async-done(((f32[256,512]{1,0:T(8,128)}), f32[64,512]{1,0:T(8,128)}) %reduce-scatter.19.cloned.1.call-update) | async-done | bytes 131088 | tf_op jit(solution)/shard_map/reduce_scatter | solution.py:85
  167.9 5.8 %all_gather.7 = bf16[256,512]{1,0:T(8,128)(2,1)S(1)} all-gather(bf16[64,512]{1,0:T(8,128)(2,1)S(1)} %add_convert_fusion), channel_id=1, replica_groups=mesh['grp'=2,'tp'=4,'dp'=4] {'tp'}, dimensions={0}, use_global_device_ids=true | all-gather | bytes 327680 | tf_op jit(solution)/shard_map/all_gather | solution.py:51
  177.2 2.2 fusion.28
  179.5 11.7 %psum.15 = f32[256]{0:T(256)S(1)} all-reduce(f32[256]{0:T(256)S(1)} %fusion.18), channel_id=1, replica_groups=mesh['grp'=2,'tp'=4,'dp'=4] {'dp'}, use_global_device_ids=true, to_apply=%region_9.10 | all-reduce | flops 256 | bytes 2048 | tf_op jit(solution)/shard_map/psum | solution.py:54
  191.3 5.6 %reduce-scatter.23.cloned.1.call-done = f32[64,512]{1,0:T(8,128)} async-done(((f32[256,512]{1,0:T(8,128)}), f32[64,512]{1,0:T(8,128)}) %reduce-scatter.23.cloned.1.call-update) | async-done | bytes 131088 | tf_op jit(solution)/shard_map/reduce_scatter | solution.py:65
  196.9 22.4 %reduce-scatter.25.cloned.1.call-done = f32[64,512]{1,0:T(8,128)} async-done(((f32[256,512]{1,0:T(8,128)}), f32[64,512]{1,0:T(8,128)}) %reduce-scatter.25.cloned.1.call-update) | async-done | bytes 131088 | tf_op jit(solution)/shard_map/reduce_scatter | solution.py:65
  219.2 22.4 %reduce-scatter.27.cloned.1.call-done = f32[64,512]{1,0:T(8,128)} async-done(((f32[256,512]{1,0:T(8,128)}), f32[64,512]{1,0:T(8,128)}) %reduce-scatter.27.cloned.1.call-update) | async-done | bytes 131088 | tf_op jit(solution)/shard_map/reduce_scatter | solution.py:65
  241.6 22.4 %reduce-scatter.21.cloned.1.call-done = f32[64,512]{1,0:T(8,128)} async-done(((f32[256,512]{1,0:T(8,128)}), f32[64,512]{1,0:T(8,128)}) %reduce-scatter.21.cloned.1.call-update) | async-done | bytes 131088 | tf_op jit(solution)/shard_map/reduce_scatter | solution.py:65
  265.6 22.5 %fusion.1 = f32[64,4,1,128]{3,2,1,0:T(1,128)S(1)} fusion(f32[64,4,128,1]{2,3,1,0:T(1,128)S(1)} %bitcast.83, f32[2,64,4,128,128]{4,3,2,1,0:T(8,128)} %param.13, f32[64,4,128]{2,1,0:T(4,128)S(1)} %mul.349, f32[64,4,128]{2,1,0:T(4,128)S(1)} %mul.346, f32[64,4,128]{2,1,0:T(4,128)S(1)} %mul.342), kind=kOutput, calls=%fused_computation.3 | convolution fusion | flops 62914560 | bytes 17432576 | tf_op jit(solution)/shard_map/bhk,bhkv->bhv/dot_general | solution.py:22
  289.2 3.4 all-to-all-start.1
  292.7 23.0 %multiply_add_fusion.1 = (f32[1,64,4,128,128]{4,3,2,1,0:T(8,128)}, f32[1,64,4,128,128]{4,3,2,1,0:T(8,128)}) fusion(f32[2,64,4,128,128]{4,3,2,1,0:T(8,128)} %param.13, f32[64,4,128]{2,1,0:T(4,128)S(1)} %copy-done.9, f32[64,4,128]{2,1,0:T(4,128)S(1)} %copy-done.7, f32[64,4,128]{2,1,0:T(4,128)S(1)} %copy-done.5, f32[64,4,128]{2,1,0:T(4,128)S(1)} %mul.349, ...), kind=kLoop, calls=%fused_computation.8 | loop fusion | flops 25165824 | bytes 67895296 | tf_op jit(solution)/shard_map/add | solution.py:21
  316.8 23.4 %pad_maximum_fusion = f32[2,64,4,128,128]{4,3,2,1,0:T(8,128)} fusion(f32[1,64,4,128,128]{4,3,2,1,0:T(8,128)} %get-tuple-element.7, f32[1,64,4,128,128]{4,3,2,1,0:T(8,128)} %get-tuple-element.6), kind=kLoop, calls=%fused_computation | loop fusion | flops 8388608 | bytes 67108864 | tf_op jit(solution)/shard_map/stack | solution.py:95
  (88 shorter events, 18.8 us)
Async XLA Ops:
  7.2 33.7 %reduce-scatter.13.cloned.1.call-start = ((), (), s32[]{:S(2)}) async-start(), calls=%async_computation.13 | async-start | bytes 655360 | tf_op jit(solution)/shard_map/reduce_scatter | solution.py:65
  17.6 45.8 %reduce-scatter.15.cloned.1.call-start = ((), (), s32[]{:S(2)}) async-start(), calls=%async_computation.14 | async-start | bytes 655360 | tf_op jit(solution)/shard_map/reduce_scatter | solution.py:65
  19.8 66.0 %reduce-scatter.17.cloned.1.call-start = ((), (), s32[]{:S(2)}) async-start(), calls=%async_computation.15 | async-start | bytes 655360 | tf_op jit(solution)/shard_map/reduce_scatter | solution.py:65
  22.0 86.0 %reduce-scatter.11.cloned.1.call-start = ((), (), s32[]{:S(2)}) async-start(), calls=%async_computation.12 | async-start | bytes 655360 | tf_op jit(solution)/shard_map/reduce_scatter | solution.py:65
  24.2 142.7 %reduce-scatter.19.cloned.1.call-start = ((), (), s32[]{:S(2)}) async-start(), calls=%async_computation.16 | async-start | bytes 655360 | tf_op jit(solution)/shard_map/reduce_scatter | solution.py:85
  37.2 73.7 %copy-start.11 = (f32[64]{0:T(128)}, f32[64]{0:T(128)S(1)}, u32[]{:S(2)}) copy-start(f32[64]{0:T(128)S(1)} %multiply_log_fusion) | copy-start | bytes 772
  109.3 24.6 %copy-start.4 = (f32[64,4,128]{2,1,0:T(4,128)}, f32[64,4,128]{2,1,0:T(4,128)S(1)}, u32[]{:S(2)}) copy-start(f32[64,4,128]{2,1,0:T(4,128)S(1)} %mul.309) | copy-start | bytes 393220
  109.4 24.6 %copy-start.6 = (f32[64,4,128]{2,1,0:T(4,128)}, f32[64,4,128]{2,1,0:T(4,128)S(1)}, u32[]{:S(2)}) copy-start(f32[64,4,128]{2,1,0:T(4,128)S(1)} %mul.313) | copy-start | bytes 393220
  109.4 36.9 %copy-start.8 = (f32[64,4,128]{2,1,0:T(4,128)}, f32[64,4,128]{2,1,0:T(4,128)S(1)}, u32[]{:S(2)}) copy-start(f32[64,4,128]{2,1,0:T(4,128)S(1)} %mul.316) | copy-start | bytes 393220
  110.9 22.9 %copy-start.13 = (f32[128]{0:T(128)S(1)}, f32[128]{0:T(128)}, u32[]{:S(2)}) copy-start(f32[128]{0:T(128)} %get-tuple-element.19) | copy-start | bytes 1540
  110.9 62.8 %copy-start = (bf16[2,512,512]{2,1,0:T(8,128)(2,1)S(1)}, bf16[2,512,512]{2,1,0:T(8,128)(2,1)}, u32[]{:S(2)}) copy-start(bf16[2,512,512]{2,1,0:T(8,128)(2,1)} %param.17) | copy-start | bytes 3145732
  110.9 64.0 %copy-start.1 = (bf16[2,512,512]{2,1,0:T(8,128)(2,1)S(1)}, bf16[2,512,512]{2,1,0:T(8,128)(2,1)}, u32[]{:S(2)}) copy-start(bf16[2,512,512]{2,1,0:T(8,128)(2,1)} %param.18) | copy-start | bytes 3145732
  110.9 65.1 %copy-start.2 = (bf16[2,512,512]{2,1,0:T(8,128)(2,1)S(1)}, bf16[2,512,512]{2,1,0:T(8,128)(2,1)}, u32[]{:S(2)}) copy-start(bf16[2,512,512]{2,1,0:T(8,128)(2,1)} %param.19) | copy-start | bytes 3145732
  146.3 50.6 %reduce-scatter.23.cloned.1.call-start = ((), (), s32[]{:S(2)}) async-start(), calls=%async_computation.18 | async-start | bytes 655360 | tf_op jit(solution)/shard_map/reduce_scatter | solution.py:65
  174.8 44.5 %reduce-scatter.25.cloned.1.call-start = ((), (), s32[]{:S(2)}) async-start(), calls=%async_computation.19 | async-start | bytes 655360 | tf_op jit(solution)/shard_map/reduce_scatter | solution.py:65
  175.9 65.7 %reduce-scatter.27.cloned.1.call-start = ((), (), s32[]{:S(2)}) async-start(), calls=%async_computation.20 | async-start | bytes 655360 | tf_op jit(solution)/shard_map/reduce_scatter | solution.py:65
  177.1 86.9 %reduce-scatter.21.cloned.1.call-start = ((), (), s32[]{:S(2)}) async-start(), calls=%async_computation.17 | async-start | bytes 655360 | tf_op jit(solution)/shard_map/reduce_scatter | solution.py:65
  179.3 109.0 %copy-start.12 = (f32[128]{0:T(128)S(1)}, f32[128]{0:T(128)}, u32[]{:S(2)}) copy-start(f32[128]{0:T(128)} %get-tuple-element.18) | copy-start | bytes 1540
  264.0 28.7 %copy-start.5 = (f32[64,4,128]{2,1,0:T(4,128)S(1)}, f32[64,4,128]{2,1,0:T(4,128)}, u32[]{:S(2)}) copy-start(f32[64,4,128]{2,1,0:T(4,128)} %copy-done.4) | copy-start | bytes 393220
  264.0 28.7 %copy-start.7 = (f32[64,4,128]{2,1,0:T(4,128)S(1)}, f32[64,4,128]{2,1,0:T(4,128)}, u32[]{:S(2)}) copy-start(f32[64,4,128]{2,1,0:T(4,128)} %copy-done.6) | copy-start | bytes 393220
  264.1 28.7 %copy-start.9 = (f32[64,4,128]{2,1,0:T(4,128)S(1)}, f32[64,4,128]{2,1,0:T(4,128)}, u32[]{:S(2)}) copy-start(f32[64,4,128]{2,1,0:T(4,128)} %copy-done.8) | copy-start | bytes 393220
  289.2 26.5 %all-to-all-start.1 = ((bf16[4,64,512]{2,1,0:T(8,128)(2,1)}), bf16[4,64,512]{2,1,0:T(8,128)(2,1)S(1)}, u32[]{:S(2)}, u32[]{:S(2)}) async-start(bf16[4,64,512]{2,1,0:T(8,128)(2,1)} %stack.7), calls=%async_computation.10 | async-start | bytes 524288 | tf_op jit(solution)/shard_map/all_to_all | solution.py:82
  292.6 23.1 %copy-start.3 = (bf16[2,512,512]{2,1,0:T(8,128)(2,1)S(1)}, bf16[2,512,512]{2,1,0:T(8,128)(2,1)}, u32[]{:S(2)}) copy-start(bf16[2,512,512]{2,1,0:T(8,128)(2,1)} %param.20) | copy-start | bytes 3145732
  292.7 47.6 %reduce-scatter.29.cloned.1.call-start = ((), (), s32[]{:S(2)}) async-start(), calls=%async_computation.21 | async-start | bytes 655360 | tf_op jit(solution)/shard_map/reduce_scatter | solution.py:85
  (1 other events, 22.9 us)
Sparse Core Ops, SparseCore 0:
  17.7 23.1 reduce-scatter.12
  43.2 20.1 reduce-scatter.14
  65.6 20.1 reduce-scatter.16
  87.9 20.0 reduce-scatter.10
  146.4 20.4 reduce-scatter.18
  174.9 21.9 reduce-scatter.22
  199.2 20.0 reduce-scatter.24
  221.5 20.0 reduce-scatter.26
  243.9 20.0 reduce-scatter.20
  317.0 22.8 reduce-scatter.28
